TPU v7x, 128 devices: a whole 4x4x4 slice. The times are simulated.
128 devices in a mesh: sp: 16 (over z, y), dp: 8 (over x, core).
Axes of the slice: x: 4, y: 4, z: 4, core: 2. Of those that a mesh axis runs over, the one named last changes fastest.
Arguments:
- inputs: bfloat16 [8, 3072, 2048], P('dp', 'sp'), may hold values from -6 to 6
- in_gain: float32 [2048], replicated, may hold values from 0.1 to 1.9
- w_query: bfloat16 [2048, 1024], P('dp', 'sp'), may hold values from -0.125 to 0.125
- w_key: bfloat16 [2048, 256], P('dp', 'sp'), may hold values from -0.375 to 0.375
- w_value: bfloat16 [2048, 256], P('dp', 'sp'), may hold values from -0.125 to 0.125
- key_bias: float32 [8, 3072, 16], P('dp', None, 'sp'), may hold values from -20 to 0
- out_gain: float32 [1024], replicated, may hold values from 0.1 to 1.9
- w_out: bfloat16 [1024, 2048], P('sp', 'dp'), may hold values from -0.1875 to 0.1875
Outputs:
- mixed: bfloat16 [8, 3072, 2048], P('dp', 'sp')
All inputs are finite; a program needn't handle non-finite values.
Results may differ from a plain program's by a relative error of at most 0.012.
The roundings to bfloat16 on the way count: a program that leaves them out, or rounds other values in their place, can miss the bound.
Values may be sent and summed in bfloat16 or wider, within the bound.
A program may use at most 128 MiB of HBM per device.

v0:
```python
import jax
import jax.numpy as jnp
from jax import lax
from jax.sharding import PartitionSpec as P

HEAD_DIM = 64
norm_eps = 1e-06


def rows_first(arrays, axis, dims):
    turned = [jnp.moveaxis(a, dim, 0) for a, dim in zip(arrays, dims)]
    both = jnp.concatenate([t.reshape(len(t), -1) for t in turned], axis=1)
    whole, at, finished = (lax.all_gather(both, axis, axis=0, tiled=True), 0, [])
    for t, dim in zip(turned, dims):
        slab = whole[:, at : at + t[0].size].reshape(-1, *t.shape[1:])
        finished.append(jnp.moveaxis(slab, 0, dim))
        at += t[0].size
    return tuple(finished)


def sent_together(arrays, axis, split_dim, concat_dim, along):
    ends, at = ([], 0)
    for a in arrays[:-1]:
        at += a.shape[along]
        ends.append(at)
    both = jnp.concatenate(arrays, axis=along)
    return tuple(
        jnp.split(
            lax.all_to_all(both, axis, split_axis=split_dim, concat_axis=concat_dim, tiled=True),
            ends,
            axis=along,
        )
    )


def body(inputs, in_gain, w_query, w_key, w_value, key_bias, out_gain, w_out):
    width_sp = lax.axis_size("sp")
    own_index = lax.axis_index("sp")
    wide = inputs[0].astype(jnp.float32)
    normed_rows = (
        wide * lax.rsqrt(jnp.mean(wide * wide, axis=-1, keepdims=True) + norm_eps) * in_gain
    ).astype(jnp.bfloat16)
    local_rows = normed_rows.shape[0]
    w_query, w_key, w_value, w_out = rows_first(
        (w_query, w_key, w_value, w_out), "dp", (0, 0, 0, 1)
    )
    w_key, w_value = rows_first((w_key, w_value), "sp", (1, 1))
    keys = jnp.dot(normed_rows, w_key, preferred_element_type=jnp.float32).astype(jnp.bfloat16)
    values = jnp.dot(normed_rows, w_value, preferred_element_type=jnp.float32).astype(jnp.bfloat16)
    queries = jnp.dot(
        normed_rows,
        lax.all_gather(w_query, "sp", axis=1, tiled=True),
        preferred_element_type=jnp.float32,
    ).astype(jnp.bfloat16)
    heads_here = key_bias.shape[2]
    kv_heads = keys.shape[1] // HEAD_DIM
    spread = width_sp // kv_heads
    query_slots = queries.reshape(local_rows, width_sp, heads_here * HEAD_DIM)
    key_copies = jnp.repeat(keys.reshape(local_rows, kv_heads, HEAD_DIM), spread, axis=1)
    value_copies = jnp.repeat(values.reshape(local_rows, kv_heads, HEAD_DIM), spread, axis=1)
    query_all, key_all, value_all = sent_together(
        (query_slots, key_copies, value_copies), "sp", 1, 0, 2
    )
    keys_head = key_all[:, 0, :]
    values_head = value_all[:, 0, :]
    length_all = query_all.shape[0]
    bias_here = key_bias[0].T
    block = min(512, length_all)
    pieces = []
    for index in range(length_all // block):
        start = index * block
        end = start + block
        logits = jnp.einsum(
            "thd,sd->hts", query_all[start:end], keys_head[:end], preferred_element_type=jnp.float32
        )
        logits = logits * HEAD_DIM ** (-0.5) + bias_here[:, None, :end]
        rows = start + jnp.arange(block, dtype=jnp.int32)[:, None]
        columns = jnp.arange(end, dtype=jnp.int32)[None, :]
        strict = (columns < rows)[None, :, :]
        log_keep = jnp.where(strict, jax.nn.log_sigmoid(-logits), jnp.float32(0.0))
        log_rest = lax.cumsum(log_keep, axis=2, reverse=True) - log_keep
        sticks = jnp.where(
            strict, jnp.exp(jax.nn.log_sigmoid(logits) + log_rest), jnp.float32(0.0)
        ).astype(jnp.bfloat16)
        pieces.append(
            jnp.einsum("hts,sd->thd", sticks, values_head[:end], preferred_element_type=jnp.float32)
        )
    attended = jnp.concatenate(pieces, axis=0)
    gains = lax.dynamic_slice_in_dim(
        out_gain, own_index * heads_here * HEAD_DIM, heads_here * HEAD_DIM, 0
    )
    scaled = attended * lax.rsqrt(jnp.mean(attended * attended, axis=-1, keepdims=True) + norm_eps)
    head_out = (scaled * gains.reshape(heads_here, HEAD_DIM)).astype(jnp.bfloat16)
    returned = lax.all_to_all(head_out, "sp", split_axis=0, concat_axis=1, tiled=True)
    returned = returned.reshape(local_rows, width_sp * heads_here * HEAD_DIM)
    mixed = jnp.dot(
        returned,
        lax.all_gather(w_out, "sp", axis=0, tiled=True),
        preferred_element_type=jnp.float32,
    )
    return mixed.astype(jnp.bfloat16)[None]


def solution(mesh):
    placed = (
        P("dp", "sp", None),
        P(),
        P("dp", "sp"),
        P("dp", "sp"),
        P("dp", "sp"),
        P("dp", None, "sp"),
        P(),
        P("sp", "dp"),
    )
    return jax.shard_map(
        body, mesh=mesh, in_specs=placed, out_specs=P("dp", "sp", None), check_vma=False
    )
```

profile of v0, /device:TPU:0, one launch (start us, length us, event | category | flops | bytes accessed | tf_op | source)
XLA Modules:
  0.0 349.7 jit_solution(17781443614021492482)
XLA Ops:
  6.5 0.9 pad_maximum_fusion.2
  7.4 13.7 %all_gather.12 = bf16[2048,160]{0,1:T(8,128)(2,1)S(1)} all-gather(bf16[256,160]{0,1:T(8,128)(2,1)S(1)} %pad_maximum_fusion.2), channel_id=1, replica_groups=mesh['sp'=16,'dp'=8] {'dp'}, dimensions={0}, use_global_device_ids=true | all-gather | bytes 737280 | tf_op jit(solution)/shard_map/all_gather | solution.py:13
  21.1 0.7 pad_maximum_fusion.1
  21.9 0.8 slice_bitcast_fusion.8
  23.0 45.8 %all-gather.6.cloned.1.call-done = bf16[256,4096]{1,0:T(8,128)(2,1)} async-done(((bf16[16,4096]{1,0:T(8,128)(2,1)}), bf16[256,4096]{1,0:T(8,128)(2,1)}) %all-gather.6.cloned.1.call-update) | async-done | bytes 2097168 | tf_op jit(solution)/shard_map/all_gather | solution.py:13
  68.8 1.9 convolution_convert_fusion.2
  71.4 50.3 %all-gather.4.cloned.1.call-done = bf16[2048,1024]{0,1:T(8,128)(2,1)} async-done(((bf16[2048,64]{0,1:T(8,128)(2,1)}), bf16[2048,1024]{0,1:T(8,128)(2,1)}) %all-gather.4.cloned.1.call-update) | async-done | bytes 4194320 | tf_op jit(solution)/shard_map/all_gather | solution.py:52
  121.7 3.7 %convolution_convert_fusion.1 = bf16[192,1024]{1,0:T(8,128)(2,1)S(1)} fusion(bf16[2048,1024]{0,1:T(8,128)(2,1)} %all-gather.4.cloned.1.call-done, bf16[1,192,2048]{2,1,0:T(8,128)(2,1)S(1)} %copy-done.4, f32[2048]{0:T(1024)S(1)} %copy-done.7, f32[192]{0:T(256)S(1)} %add_rsqrt_fusion.1), kind=kOutput, calls=%fused_computation.128 | convolution fusion | flops 807075840 | bytes 5382912 | tf_op jit(solution)/shard_map/dot_general | solution.py:50
  125.8 1.4 pad_maximum_fusion
  127.2 5.3 %all-to-all-start = ((bf16[192,16,192]{0,2,1:T(8,128)(2,1)}), bf16[192,16,192]{0,2,1:T(8,128)(2,1)S(1)}, u32[]{:S(2)}, u32[]{:S(2)}) async-start(bf16[192,16,192]{0,2,1:T(8,128)(2,1)} %pad_maximum_fusion), calls=%async_computation | async-start | bytes 3145728 | tf_op jit(solution)/shard_map/all_to_all | solution.py:29
  132.5 0.6 all-gather.8.cloned.1.call-start
  133.3 0.8 dynamic_slice.3
  134.2 23.7 %all-to-all-done = bf16[192,16,192]{0,2,1:T(8,128)(2,1)S(1)} async-done(((bf16[192,16,192]{0,2,1:T(8,128)(2,1)}), bf16[192,16,192]{0,2,1:T(8,128)(2,1)S(1)}, u32[]{:S(2)}, u32[]{:S(2)}) %all-to-all-start) | async-done | bytes 1179680 | tf_op jit(solution)/shard_map/all_to_all | solution.py:29
  157.9 0.9 copy.59
  158.7 1.7 all_to_all.27
  160.5 1.6 fusion.116
  162.1 4.8 %fusion.121 = f32[1,512,4,128]{1,2,3,0:T(4,128)S(1)} fusion(f32[1,512,4,128]{1,3,2,0:T(8,128)S(1)} %bitcast.409), kind=kOutput, calls=%fused_computation.155 | output fusion | flops 33292288 | bytes 2097152 | tf_op jit(solution)/shard_map/reduce-window
  166.9 1.3 copy.61
  168.2 2.9 fusion.66
  171.0 5.2 %fusion.74 = f32[1,512,8,128]{1,2,3,0:T(8,128)S(1)} fusion(f32[1,512,8,128]{1,3,2,0:T(8,128)S(1)} %bitcast.404), kind=kOutput, calls=%fused_computation.113 | output fusion | flops 66584576 | bytes 4194304 | tf_op jit(solution)/shard_map/reduce-window.2
  176.2 2.6 copy.63
  178.8 4.1 %fusion.53 = (f32[1,512,1536]{1,2,0:T(8,128)S(1)}, f32[1,512,1536]{1,2,0:T(8,128)}) fusion(s32[512]{0:T(512)S(1)} %iota_add_fusion.3, f32[1536]{0:T(1024)S(1)} %slice_reduce_fusion.1, bf16[3072,1,192]{0,2,1:T(8,128)(2,1)S(1)} %all_to_all.27), kind=kOutput, calls=%fused_computation.82 | convolution fusion | flops 109314048 | bytes 6563840 | tf_op jit(solution)/shard_map/thd,sd->hts/dot_general | solution.py:73
  182.9 10.1 %fusion.42 = f32[1,512,12,128]{1,2,3,0:T(8,128)S(1)} fusion(f32[1,512,12,128]{1,3,2,0:T(8,128)S(1)} %bitcast.402), kind=kOutput, calls=%fused_computation.69 | output fusion | flops 99876864 | bytes 6291456 | tf_op jit(solution)/shard_map/reduce-window.4
  193.0 1.8 copy.65
  194.9 6.1 %fusion.34 = (f32[1,512,2048]{1,2,0:T(8,128)S(1)}, f32[2048,512]{1,0:T(8,128)}) fusion(f32[2048]{0:T(1024)S(1)} %bitcast.419, s32[512]{0:T(512)S(1)} %iota_add_fusion.2, bf16[3072,1,192]{0,2,1:T(8,128)(2,1)} %copy-done.1), kind=kOutput, calls=%fused_computation.56 | convolution fusion | flops 145752064 | bytes 8726528 | tf_op jit(solution)/shard_map/thd,sd->hts/dot_general | solution.py:73
  201.0 10.3 %fusion.40 = f32[1,512,16,128]{1,2,3,0:T(8,128)S(1)} fusion(f32[1,512,16,128]{1,3,2,0:T(8,128)S(1)} %bitcast.401), kind=kOutput, calls=%fused_computation.67 | output fusion | flops 133169152 | bytes 8388608 | tf_op jit(solution)/shard_map/reduce-window.6
  211.3 4.4 %copy.67 = f32[1,512,16,128]{1,3,2,0:T(8,128)} copy(f32[1,512,16,128]{1,2,3,0:T(8,128)S(1)} %fusion.40) | data formatting | bytes 8388608 | tf_op jit(solution)/shard_map/reduce-window.6
  215.8 7.1 %fusion.22 = (f32[1,512,2560]{1,2,0:T(8,128)S(1)}, f32[2560,512,1]{1,0,2:T(8,128)}) fusion(s32[512]{0:T(512)S(1)} %iota_add_fusion.1, f32[2560]{0:T(1024)S(1)} %slice_reduce_fusion, bf16[3072,1,192]{0,2,1:T(8,128)(2,1)} %copy-done.1), kind=kOutput, calls=%fused_computation.38 | convolution fusion | flops 182190080 | bytes 10891264 | tf_op jit(solution)/shard_map/thd,sd->hts/dot_general | solution.py:73
  222.9 15.6 %fusion.14 = f32[1,512,20,128]{1,2,3,0:T(8,128)S(1)} fusion(f32[1,512,20,128]{1,3,2,0:T(8,128)S(1)} %bitcast.400), kind=kOutput, calls=%fused_computation.27 | output fusion | flops 166461440 | bytes 10485760 | tf_op jit(solution)/shard_map/reduce-window.8
  238.5 5.4 %copy.69 = f32[1,512,20,128]{1,3,2,0:T(8,128)} copy(f32[1,512,20,128]{1,2,3,0:T(8,128)S(1)} %fusion.14) | data formatting | bytes 10485760 | tf_op jit(solution)/shard_map/reduce-window.8
  244.0 8.2 %fusion.6 = (f32[1,512,3072]{1,2,0:T(8,128)S(1)}, f32[3072,512]{1,0:T(8,128)}) fusion(f32[3072]{0:T(1024)S(1)} %bitcast.417, s32[512]{0:T(512)S(1)} %iota_add_fusion, bf16[3072,1,192]{0,2,1:T(8,128)(2,1)} %copy-done.1), kind=kOutput, calls=%fused_computation.14 | convolution fusion | flops 218628096 | bytes 13056000 | tf_op jit(solution)/shard_map/thd,sd->hts/dot_general | solution.py:73
  252.2 15.3 %fusion.12 = f32[1,512,24,128]{1,2,3,0:T(8,128)S(1)} fusion(f32[1,512,24,128]{1,3,2,0:T(8,128)S(1)} %bitcast.398), kind=kOutput, calls=%fused_computation.25 | output fusion | flops 199753728 | bytes 12582912 | tf_op jit(solution)/shard_map/reduce-window.10
  267.5 6.3 %copy.71 = f32[1,512,24,128]{1,3,2,0:T(8,128)} copy(f32[1,512,24,128]{1,2,3,0:T(8,128)S(1)} %fusion.12) | data formatting | bytes 12582912 | tf_op jit(solution)/shard_map/reduce-window.10
  274.0 2.6 fusion.114
  276.7 5.8 %fusion.64 = bf16[1,512,1024]{1,2,0:T(8,128)(2,1)S(1)} fusion(f32[1,512,8,128]{1,3,2,0:T(8,128)} %copy.63, f32[1024,512]{1,0:T(8,128)} %get-tuple-element.12, f32[512,8]{0,1:T(8,128)S(1)} %slice_bitcast_fusion.47, f32[1024]{0:T(1024)S(1)} %bitcast.423, s32[512]{0:T(512)S(1)} %iota_add_fusion.4), kind=kLoop, calls=%fused_computation.98 | loop fusion | flops 12582912 | bytes 5265408 | tf_op jit(solution)/shard_map/convert_element_type | solution.py:84
  282.5 6.4 %fusion.51 = bf16[1,512,1536]{1,2,0:T(8,128)(2,1)S(1)} fusion(f32[1,512,12,128]{1,3,2,0:T(8,128)S(1)} %copy.65, f32[1,512,1536]{1,2,0:T(8,128)} %get-tuple-element.14, f32[512,12]{0,1:T(8,128)S(1)} %slice_bitcast_fusion.45, s32[512]{0:T(512)S(1)} %iota_add_fusion.3), kind=kLoop, calls=%fused_computation.80 | loop fusion | flops 17301504 | bytes 7890944 | tf_op jit(solution)/shard_map/convert_element_type | solution.py:84
  288.9 7.3 %fusion.32 = bf16[1,512,2048]{1,2,0:T(8,128)(2,1)S(1)} fusion(f32[1,512,16,128]{1,3,2,0:T(8,128)S(1)} %copy-done, f32[2048,512]{1,0:T(8,128)S(1)} %copy-done.3, f32[512,16]{0,1:T(8,128)S(1)} %slice_bitcast_fusion.43, f32[2048]{0:T(1024)S(1)} %bitcast.420, s32[512]{0:T(512)S(1)} %iota_add_fusion.2), kind=kLoop, calls=%fused_computation.54 | loop fusion | flops 25165824 | bytes 10528768 | tf_op jit(solution)/shard_map/convert_element_type | solution.py:84
  296.3 9.8 %fusion.20 = bf16[1,512,2560]{1,2,0:T(8,128)(2,1)S(1)} fusion(f32[1,512,20,128]{1,3,2,0:T(8,128)S(1)} %bitcast.395, f32[2560,512,1]{1,0,2:T(8,128)} %get-tuple-element.18, f32[512,20]{0,1:T(8,128)S(1)} %slice_bitcast_fusion.41, s32[512]{0:T(512)S(1)} %iota_add_fusion.1), kind=kLoop, calls=%fused_computation.36 | loop fusion | flops 28835840 | bytes 13150208 | tf_op jit(solution)/shard_map/convert_element_type | solution.py:84
  306.2 10.9 %fusion.4 = bf16[1,512,3072]{1,2,0:T(8,128)(2,1)S(1)} fusion(f32[1,512,24,128]{1,3,2,0:T(8,128)S(1)} %bitcast.393, f32[3072,512]{1,0:T(8,128)S(1)} %bitcast.397, f32[512,24]{0,1:T(8,128)S(1)} %slice_bitcast_fusion.39, f32[3072]{0:T(1024)S(1)} %bitcast.418, s32[512]{0:T(512)S(1)} %iota_add_fusion), kind=kLoop, calls=%fused_computation.12 | loop fusion | flops 37748736 | bytes 15792128 | tf_op jit(solution)/shard_map/convert_element_type | solution.py:84
  318.5 0.6 fusion.93
  319.0 0.7 fusion.107
  319.9 0.6 broadcast.275
  320.5 0.9 reduce.5
  322.4 13.3 %all_to_all.33 = bf16[16,2,6144]{2,1,0:T(2,128)(2,1)S(1)} all-to-all(bf16[16,2,6144]{2,1,0:T(2,128)(2,1)S(1)} %reshape.777), channel_id=1, replica_groups=mesh['sp'=16,'dp'=8] {'sp'}, dimensions={0} | all-to-all | bytes 786432 | tf_op jit(solution)/shard_map/all_to_all | solution.py:94
  335.7 0.8 reshape.778
  336.5 1.5 copy.73
  338.0 0.6 all_to_all.29
  338.8 4.1 %fusion.59 = bf16[1,192,2048]{2,1,0:T(8,128)(2,1)} fusion(bf16[192,1024]{0,1:T(8,128)(2,1)S(1)} %bitcast.408, bf16[1024,2048]{1,0:T(8,128)(2,1)} %all-gather.8.cloned.1.call-done), kind=kOutput, calls=%fused_computation.93 | convolution fusion | flops 805699584 | bytes 5373952 | tf_op jit(solution)/shard_map/dot_general | solution.py:96
  (84 shorter events, 4.9 us)
Async XLA Ops:
  6.5 16.2 %copy-start.4 = (bf16[1,192,2048]{2,1,0:T(8,128)(2,1)S(1)}, bf16[1,192,2048]{2,1,0:T(8,128)(2,1)}, u32[]{:S(2)}) copy-start(bf16[1,192,2048]{2,1,0:T(8,128)(2,1)} %param.8) | copy-start | bytes 2359300
  6.5 62.3 %copy-start.7 = (f32[2048]{0:T(1024)S(1)}, f32[2048]{0:T(1024)}, u32[]{:S(2)}) copy-start(f32[2048]{0:T(1024)} %param.9) | copy-start | bytes 24580
  6.5 62.2 %all-gather.6.cloned.1.call-start = ((), (), s32[]{:S(2)}) async-start(), calls=%async_computation.3 | async-start | bytes 2228224 | tf_op jit(solution)/shard_map/all_gather | solution.py:13
  21.8 99.9 %all-gather.4.cloned.1.call-start = ((), (), s32[]{:S(2)}) async-start(), calls=%async_computation.2 | async-start | bytes 4456448 | tf_op jit(solution)/shard_map/all_gather | solution.py:52
  68.8 2.0 copy-start.6
  125.8 7.5 %copy-start.5 = (f32[1,3072,1]{1,2,0:T(1,128)S(1)}, f32[1,3072,1]{1,2,0:T(1,128)}, u32[]{:S(2)}) copy-start(f32[1,3072,1]{1,2,0:T(1,128)} %param.13) | copy-start | bytes 36868
  127.2 30.6 %all-to-all-start = ((bf16[192,16,192]{0,2,1:T(8,128)(2,1)}), bf16[192,16,192]{0,2,1:T(8,128)(2,1)S(1)}, u32[]{:S(2)}, u32[]{:S(2)}) async-start(bf16[192,16,192]{0,2,1:T(8,128)(2,1)} %pad_maximum_fusion), calls=%async_computation | async-start | bytes 3145728 | tf_op jit(solution)/shard_map/all_to_all | solution.py:29
  132.5 206.2 %all-gather.8.cloned.1.call-start = ((), (), s32[]{:S(2)}) async-start(), calls=%async_computation.4 | async-start | bytes 4456448 | tf_op jit(solution)/shard_map/all_gather | solution.py:98
  160.4 18.4 %copy-start.1 = (bf16[3072,1,192]{0,2,1:T(8,128)(2,1)}, bf16[3072,1,192]{0,2,1:T(8,128)(2,1)S(1)}, u32[]{:S(2)}) copy-start(bf16[3072,1,192]{0,2,1:T(8,128)(2,1)S(1)} %all_to_all.27) | copy-start | bytes 3538948
  274.0 14.8 %copy-start.3 = (f32[2048,512]{1,0:T(8,128)S(1)}, f32[2048,512]{1,0:T(8,128)}, u32[]{:S(2)}) copy-start(f32[2048,512]{1,0:T(8,128)} %get-tuple-element.16) | copy-start | bytes 12582916
  276.7 19.6 %slice-start.2 = ((s8[5242880]{0:T(1024)(128)(4,1)}), s8[4194304]{0:T(1024)(128)(4,1)S(1)}, s32[]{:S(2)}) async-start(s8[5242880]{0:T(1024)(128)(4,1)} %bitcast.394), calls=%async_computation.7 | async-start | bytes 8388608
  282.4 6.4 %copy-start = (f32[1,512,16,128]{1,3,2,0:T(8,128)S(1)}, f32[1,512,16,128]{1,3,2,0:T(8,128)}, u32[]{:S(2)}) copy-start(f32[1,512,16,128]{1,3,2,0:T(8,128)} %copy.67) | copy-start | bytes 12582916
  282.4 13.8 %slice-start.3 = ((s8[5242880]{0:T(1024)(128)(4,1)}), s8[1048576]{0:T(1024)(128)(4,1)S(1)}, s32[]{:S(2)}) async-start(s8[5242880]{0:T(1024)(128)(4,1)} %bitcast.394), calls=%async_computation.8 | async-start | bytes 2097152
  288.9 17.3 %slice-start = ((s8[6291456]{0:T(1024)(128)(4,1)}), s8[4194304]{0:T(1024)(128)(4,1)S(1)}, s32[]{:S(2)}) async-start(s8[6291456]{0:T(1024)(128)(4,1)} %bitcast.392), calls=%async_computation.5 | async-start | bytes 8388608
  288.9 17.3 %slice-start.4 = ((s8[6291456]{0:T(1024)(128)(4,1)}), s8[2097152]{0:T(1024)(128)(4,1)S(1)}, s32[]{:S(2)}) async-start(s8[6291456]{0:T(1024)(128)(4,1)} %bitcast.396), calls=%async_computation.9 | async-start | bytes 4194304
  296.2 9.9 %slice-start.1 = ((s8[6291456]{0:T(1024)(128)(4,1)}), s8[2097152]{0:T(1024)(128)(4,1)S(1)}, s32[]{:S(2)}) async-start(s8[6291456]{0:T(1024)(128)(4,1)} %bitcast.392), calls=%async_computation.6 | async-start | bytes 4194304
  296.2 9.9 %slice-start.5 = ((s8[6291456]{0:T(1024)(128)(4,1)}), s8[4194304]{0:T(1024)(128)(4,1)S(1)}, s32[]{:S(2)}) async-start(s8[6291456]{0:T(1024)(128)(4,1)} %bitcast.396), calls=%async_computation.10 | async-start | bytes 8388608
  306.2 10.9 %copy-start.2 = (bf16[3072,1,192]{0,2,1:T(8,128)(2,1)S(1)}, bf16[3072,1,192]{0,2,1:T(8,128)(2,1)}, u32[]{:S(2)}) copy-start(bf16[3072,1,192]{0,2,1:T(8,128)(2,1)} %copy-done.1) | copy-start | bytes 3538948
Sparse Core Ops, SparseCore 0:
  21.9 46.8 all-gather.5
  70.9 50.7 all-gather.3
  135.5 54.9 all-gather.7
where the time goes:
time: 353 us; the launch traced here: 350 us
  waiting for transfers between devices  120 us (34%)
  other arithmetic  109 us (31%)
  matrix products  42.7 us (12%)
  local copies, waits for them, and re-layouts  31.2 us (9%)
  blocking collectives  27 us (8%)
  between operations  14 us (4%)
  starting transfers between devices  5.9 us (2%)
    another operation x12, other arithmetic  61.8 us
    all_gather x1, waiting for transfers between devices, body(): lax.all_gather(w_query, 'sp', axis=1, tiled=True)  50.3 us
    all_gather x1, waiting for transfers between devices, rows_first(): lax.all_gather(both, axis, axis=0, tiled=True)  45.8 us
    convert_element_type x6, other arithmetic, body(): sticks = jnp.where(strict, jnp.exp(jax.nn.log_sigmoid(logits) + log_rest)...  42.8 us
    dot_general x6, matrix products, body(): jnp.einsum('thd,sd->hts', query_all[start:end], keys_head[:end], preferre...  29.9 us
    all_to_all x1, waiting for transfers between devices, sent_together(): lax.all_to_all(both, axis, split_axis=split_dim, concat_axis=concat_dim,...  23.7 us
    another operation x18, local copies, waits for them, and re-layouts  21.8 us
    all_gather x1, blocking collectives, rows_first(): lax.all_gather(both, axis, axis=0, tiled=True)  13.7 us
  transfers between devices with their start and end apart: 4, of which 3 were waited for; matrix products, arithmetic and copies ran while one was open for 48% of the time, Pallas kernels for 0%

commit v1 on v0

--- a/solution.py
+++ b/solution.py
@@ -5,6 +5,11 @@
 
 HEAD_DIM = 64
 norm_eps = 1e-06
+
+
+def gather_blocks(x, mesh_axis, dim):
+    blocks = lax.all_gather(x, mesh_axis)
+    return jnp.concatenate(blocks, axis=dim)
 
 
 def rows_first(arrays, axis, dims):
@@ -48,9 +53,7 @@
     keys = jnp.dot(normed_rows, w_key, preferred_element_type=jnp.float32).astype(jnp.bfloat16)
     values = jnp.dot(normed_rows, w_value, preferred_element_type=jnp.float32).astype(jnp.bfloat16)
     queries = jnp.dot(
-        normed_rows,
-        lax.all_gather(w_query, "sp", axis=1, tiled=True),
-        preferred_element_type=jnp.float32,
+        normed_rows, gather_blocks(w_query, "sp", 1), preferred_element_type=jnp.float32
     ).astype(jnp.bfloat16)
     heads_here = key_bias.shape[2]
     kv_heads = keys.shape[1] // HEAD_DIM

time: 353 us -> 362 us (1.025); the launches traced: 350 us -> 355 us
  local copies, waits for them, and re-layouts: 31.2 us -> 38.1 us
    unnamed x31 -> x32, local copies, waits for them, and re-layouts: 1.76 us -> 6.35 us
where the time goes in v1:
time: 362 us; the launch traced here: 355 us
  waiting for transfers between devices  120 us (33%)
  other arithmetic  109 us (30%)
  matrix products  40.5 us (11%)
  local copies, waits for them, and re-layouts  38.1 us (11%)
  blocking collectives  27 us (7%)
  between operations  14.2 us (4%)
  starting transfers between devices  5.59 us (2%)
    another operation x12, other arithmetic  61.9 us
    all_gather x1, waiting for transfers between devices, gather_blocks(): blocks = lax.all_gather(x, mesh_axis)  50.3 us
    all_gather x1, waiting for transfers between devices, rows_first(): lax.all_gather(both, axis, axis=0, tiled=True)  45.8 us
    convert_element_type x6, other arithmetic, body(): sticks = jnp.where(strict, jnp.exp(jax.nn.log_sigmoid(logits) + log_rest)...  42.8 us
    dot_general x6, matrix products, body(): jnp.einsum('thd,sd->hts', query_all[start:end], keys_head[:end], preferre...  29.9 us
    all_to_all x1, waiting for transfers between devices, sent_together(): lax.all_to_all(both, axis, split_axis=split_dim, concat_axis=concat_dim,...  23.7 us
    another operation x18, local copies, waits for them, and re-layouts  21.8 us
    all_gather x1, blocking collectives, rows_first(): lax.all_gather(both, axis, axis=0, tiled=True)  13.7 us
  transfers between devices with their start and end apart: 4, of which 3 were waited for; matrix products, arithmetic and copies ran while one was open for 48% of the time, Pallas kernels for 0%

profile of v1, /device:TPU:0, one launch (start us, length us, event | category | flops | bytes accessed | tf_op | source)
XLA Modules:
  0.0 354.7 jit_solution(16924949615118615228)
XLA Ops:
  6.5 0.9 pad_maximum_fusion.2
  7.4 13.7 %all_gather.15 = bf16[2048,160]{0,1:T(8,128)(2,1)S(1)} all-gather(bf16[256,160]{0,1:T(8,128)(2,1)S(1)} %pad_maximum_fusion.2), channel_id=1, replica_groups=mesh['sp'=16,'dp'=8] {'dp'}, dimensions={0}, use_global_device_ids=true | all-gather | bytes 737280 | tf_op jit(solution)/shard_map/all_gather | solution.py:18
  21.1 0.7 pad_maximum_fusion.1
  21.9 0.8 slice_bitcast_fusion.8
  23.0 45.8 %all-gather.5.cloned.1.call-done = bf16[256,4096]{1,0:T(8,128)(2,1)} async-done(((bf16[16,4096]{1,0:T(8,128)(2,1)}), bf16[256,4096]{1,0:T(8,128)(2,1)}) %all-gather.5.cloned.1.call-update) | async-done | bytes 2097168 | tf_op jit(solution)/shard_map/all_gather | solution.py:18
  68.8 1.9 convolution_convert_fusion.2
  71.4 50.3 %all-gather.9.cloned.1.call-done = bf16[32768,64]{0,1:T(8,128)(2,1)} async-done(((bf16[2048,64]{0,1:T(8,128)(2,1)}), bf16[32768,64]{0,1:T(8,128)(2,1)}) %all-gather.9.cloned.1.call-update) | async-done | bytes 4194320 | tf_op jit(solution)/shard_map/all_gather | solution.py:11
  121.7 4.6 %copy.95 = bf16[8,8,16,2048]{3,2,1,0:T(8,128)(2,1)S(1)} copy(bf16[8,8,16,2048]{3,1,2,0:T(8,128)(2,1)} %bitcast.419) | data formatting | bytes 8388608
  126.3 2.3 copy.75
  128.6 1.6 convolution_convert_fusion.1
  130.5 1.4 pad_maximum_fusion
  132.0 5.3 %all-to-all-start = ((bf16[192,16,192]{0,2,1:T(8,128)(2,1)}), bf16[192,16,192]{0,2,1:T(8,128)(2,1)S(1)}, u32[]{:S(2)}, u32[]{:S(2)}) async-start(bf16[192,16,192]{0,2,1:T(8,128)(2,1)} %pad_maximum_fusion), calls=%async_computation | async-start | bytes 3145728 | tf_op jit(solution)/shard_map/all_to_all | solution.py:34
  138.0 0.8 dynamic_slice.3
  138.9 23.7 %all-to-all-done = bf16[192,16,192]{0,2,1:T(8,128)(2,1)S(1)} async-done(((bf16[192,16,192]{0,2,1:T(8,128)(2,1)}), bf16[192,16,192]{0,2,1:T(8,128)(2,1)S(1)}, u32[]{:S(2)}, u32[]{:S(2)}) %all-to-all-start) | async-done | bytes 1179680 | tf_op jit(solution)/shard_map/all_to_all | solution.py:34
  162.6 0.9 copy.79
  163.5 1.7 all_to_all.27
  165.2 1.6 fusion.120
  166.8 4.8 %fusion.125 = f32[1,512,4,128]{1,2,3,0:T(4,128)S(1)} fusion(f32[1,512,4,128]{1,3,2,0:T(8,128)S(1)} %bitcast.429), kind=kOutput, calls=%fused_computation.159 | output fusion | flops 33292288 | bytes 2097152 | tf_op jit(solution)/shard_map/reduce-window
  171.6 1.3 copy.81
  172.9 2.9 fusion.66
  175.8 5.4 %fusion.74 = f32[1,512,8,128]{1,2,3,0:T(8,128)S(1)} fusion(f32[1,512,8,128]{1,3,2,0:T(8,128)S(1)} %bitcast.424), kind=kOutput, calls=%fused_computation.113 | output fusion | flops 66584576 | bytes 4194304 | tf_op jit(solution)/shard_map/reduce-window.2
  181.2 2.6 copy.83
  183.8 4.1 %fusion.53 = (f32[1,512,1536]{1,2,0:T(8,128)S(1)}, f32[1,512,1536]{1,2,0:T(8,128)}) fusion(s32[512]{0:T(512)S(1)} %iota_add_fusion.3, f32[1536]{0:T(1024)S(1)} %slice_reduce_fusion.1, bf16[3072,1,192]{0,2,1:T(8,128)(2,1)S(1)} %all_to_all.27), kind=kOutput, calls=%fused_computation.82 | convolution fusion | flops 109314048 | bytes 6563840 | tf_op jit(solution)/shard_map/thd,sd->hts/dot_general | solution.py:76
  187.8 10.1 %fusion.42 = f32[1,512,12,128]{1,2,3,0:T(8,128)S(1)} fusion(f32[1,512,12,128]{1,3,2,0:T(8,128)S(1)} %bitcast.422), kind=kOutput, calls=%fused_computation.69 | output fusion | flops 99876864 | bytes 6291456 | tf_op jit(solution)/shard_map/reduce-window.4
  197.9 1.8 copy.85
  199.9 6.1 %fusion.34 = (f32[1,512,2048]{1,2,0:T(8,128)S(1)}, f32[2048,512]{1,0:T(8,128)}) fusion(f32[2048]{0:T(1024)S(1)} %bitcast.439, s32[512]{0:T(512)S(1)} %iota_add_fusion.2, bf16[3072,1,192]{0,2,1:T(8,128)(2,1)} %copy-done.1), kind=kOutput, calls=%fused_computation.56 | convolution fusion | flops 145752064 | bytes 8726528 | tf_op jit(solution)/shard_map/thd,sd->hts/dot_general | solution.py:76
  206.0 10.2 %fusion.40 = f32[1,512,16,128]{1,2,3,0:T(8,128)S(1)} fusion(f32[1,512,16,128]{1,3,2,0:T(8,128)S(1)} %bitcast.421), kind=kOutput, calls=%fused_computation.67 | output fusion | flops 133169152 | bytes 8388608 | tf_op jit(solution)/shard_map/reduce-window.6
  216.2 4.4 %copy.87 = f32[1,512,16,128]{1,3,2,0:T(8,128)} copy(f32[1,512,16,128]{1,2,3,0:T(8,128)S(1)} %fusion.40) | data formatting | bytes 8388608 | tf_op jit(solution)/shard_map/reduce-window.6
  220.7 7.1 %fusion.22 = (f32[1,512,2560]{1,2,0:T(8,128)S(1)}, f32[2560,512,1]{1,0,2:T(8,128)}) fusion(s32[512]{0:T(512)S(1)} %iota_add_fusion.1, f32[2560]{0:T(1024)S(1)} %slice_reduce_fusion, bf16[3072,1,192]{0,2,1:T(8,128)(2,1)} %copy-done.1), kind=kOutput, calls=%fused_computation.38 | convolution fusion | flops 182190080 | bytes 10891264 | tf_op jit(solution)/shard_map/thd,sd->hts/dot_general | solution.py:76
  227.9 15.5 %fusion.14 = f32[1,512,20,128]{1,2,3,0:T(8,128)S(1)} fusion(f32[1,512,20,128]{1,3,2,0:T(8,128)S(1)} %bitcast.418), kind=kOutput, calls=%fused_computation.27 | output fusion | flops 166461440 | bytes 10485760 | tf_op jit(solution)/shard_map/reduce-window.8
  243.4 5.4 %copy.89 = f32[1,512,20,128]{1,3,2,0:T(8,128)} copy(f32[1,512,20,128]{1,2,3,0:T(8,128)S(1)} %fusion.14) | data formatting | bytes 10485760 | tf_op jit(solution)/shard_map/reduce-window.8
  248.9 8.2 %fusion.6 = (f32[1,512,3072]{1,2,0:T(8,128)S(1)}, f32[3072,512]{1,0:T(8,128)}) fusion(f32[3072]{0:T(1024)S(1)} %bitcast.437, s32[512]{0:T(512)S(1)} %iota_add_fusion, bf16[3072,1,192]{0,2,1:T(8,128)(2,1)} %copy-done.1), kind=kOutput, calls=%fused_computation.14 | convolution fusion | flops 218628096 | bytes 13056000 | tf_op jit(solution)/shard_map/thd,sd->hts/dot_general | solution.py:76
  257.1 15.3 %fusion.12 = f32[1,512,24,128]{1,2,3,0:T(8,128)S(1)} fusion(f32[1,512,24,128]{1,3,2,0:T(8,128)S(1)} %bitcast.416), kind=kOutput, calls=%fused_computation.25 | output fusion | flops 199753728 | bytes 12582912 | tf_op jit(solution)/shard_map/reduce-window.10
  272.4 6.3 %copy.91 = f32[1,512,24,128]{1,3,2,0:T(8,128)} copy(f32[1,512,24,128]{1,2,3,0:T(8,128)S(1)} %fusion.12) | data formatting | bytes 12582912 | tf_op jit(solution)/shard_map/reduce-window.10
  278.9 2.6 fusion.118
  281.5 5.8 %fusion.64 = bf16[1,512,1024]{1,2,0:T(8,128)(2,1)S(1)} fusion(f32[1,512,8,128]{1,3,2,0:T(8,128)} %copy.83, f32[1024,512]{1,0:T(8,128)} %get-tuple-element.12, f32[512,8]{0,1:T(8,128)S(1)} %slice_bitcast_fusion.47, f32[1024]{0:T(1024)S(1)} %bitcast.443, s32[512]{0:T(512)S(1)} %iota_add_fusion.4), kind=kLoop, calls=%fused_computation.98 | loop fusion | flops 12582912 | bytes 5265408 | tf_op jit(solution)/shard_map/convert_element_type | solution.py:87
  287.3 6.4 %fusion.51 = bf16[1,512,1536]{1,2,0:T(8,128)(2,1)S(1)} fusion(f32[1,512,12,128]{1,3,2,0:T(8,128)S(1)} %copy.85, f32[1,512,1536]{1,2,0:T(8,128)} %get-tuple-element.14, f32[512,12]{0,1:T(8,128)S(1)} %slice_bitcast_fusion.45, s32[512]{0:T(512)S(1)} %iota_add_fusion.3), kind=kLoop, calls=%fused_computation.80 | loop fusion | flops 17301504 | bytes 7890944 | tf_op jit(solution)/shard_map/convert_element_type | solution.py:87
  293.8 7.3 %fusion.32 = bf16[1,512,2048]{1,2,0:T(8,128)(2,1)S(1)} fusion(f32[1,512,16,128]{1,3,2,0:T(8,128)S(1)} %copy-done, f32[2048,512]{1,0:T(8,128)S(1)} %copy-done.3, f32[512,16]{0,1:T(8,128)S(1)} %slice_bitcast_fusion.43, f32[2048]{0:T(1024)S(1)} %bitcast.440, s32[512]{0:T(512)S(1)} %iota_add_fusion.2), kind=kLoop, calls=%fused_computation.54 | loop fusion | flops 25165824 | bytes 10528768 | tf_op jit(solution)/shard_map/convert_element_type | solution.py:87
  301.1 9.8 %fusion.20 = bf16[1,512,2560]{1,2,0:T(8,128)(2,1)S(1)} fusion(f32[1,512,20,128]{1,3,2,0:T(8,128)S(1)} %bitcast.412, f32[2560,512,1]{1,0,2:T(8,128)} %get-tuple-element.18, f32[512,20]{0,1:T(8,128)S(1)} %slice_bitcast_fusion.41, s32[512]{0:T(512)S(1)} %iota_add_fusion.1), kind=kLoop, calls=%fused_computation.36 | loop fusion | flops 28835840 | bytes 13150208 | tf_op jit(solution)/shard_map/convert_element_type | solution.py:87
  311.1 10.9 %fusion.4 = bf16[1,512,3072]{1,2,0:T(8,128)(2,1)S(1)} fusion(f32[1,512,24,128]{1,3,2,0:T(8,128)S(1)} %bitcast.410, f32[3072,512]{1,0:T(8,128)S(1)} %bitcast.415, f32[512,24]{0,1:T(8,128)S(1)} %slice_bitcast_fusion.39, f32[3072]{0:T(1024)S(1)} %bitcast.438, s32[512]{0:T(512)S(1)} %iota_add_fusion), kind=kLoop, calls=%fused_computation.12 | loop fusion | flops 37748736 | bytes 15792128 | tf_op jit(solution)/shard_map/convert_element_type | solution.py:87
  323.9 0.7 fusion.111
  324.8 0.6 broadcast.282
  325.4 0.9 reduce.5
  327.3 13.3 %all_to_all.33 = bf16[16,2,6144]{2,1,0:T(2,128)(2,1)S(1)} all-to-all(bf16[16,2,6144]{2,1,0:T(2,128)(2,1)S(1)} %reshape.800), channel_id=1, replica_groups=mesh['sp'=16,'dp'=8] {'sp'}, dimensions={0} | all-to-all | bytes 786432 | tf_op jit(solution)/shard_map/all_to_all | solution.py:97
  340.6 0.8 reshape.801
  341.4 1.5 copy.93
  342.9 0.6 all_to_all.29
  343.7 4.1 %fusion.59 = bf16[1,192,2048]{2,1,0:T(8,128)(2,1)} fusion(bf16[192,1024]{0,1:T(8,128)(2,1)S(1)} %bitcast.428, bf16[1024,2048]{1,0:T(8,128)(2,1)} %all-gather.7.cloned.1.call-done), kind=kOutput, calls=%fused_computation.93 | convolution fusion | flops 805699584 | bytes 5373952 | tf_op jit(solution)/shard_map/dot_general | solution.py:99
  (86 shorter events, 6.1 us)
Async XLA Ops:
  6.5 16.2 %copy-start.4 = (bf16[1,192,2048]{2,1,0:T(8,128)(2,1)S(1)}, bf16[1,192,2048]{2,1,0:T(8,128)(2,1)}, u32[]{:S(2)}) copy-start(bf16[1,192,2048]{2,1,0:T(8,128)(2,1)} %param.8) | copy-start | bytes 2359300
  6.5 62.3 %copy-start.7 = (f32[2048]{0:T(1024)S(1)}, f32[2048]{0:T(1024)}, u32[]{:S(2)}) copy-start(f32[2048]{0:T(1024)} %param.9) | copy-start | bytes 24580
  6.5 62.2 %all-gather.5.cloned.1.call-start = ((), (), s32[]{:S(2)}) async-start(), calls=%async_computation.2 | async-start | bytes 2228224 | tf_op jit(solution)/shard_map/all_gather | solution.py:18
  21.8 99.9 %all-gather.9.cloned.1.call-start = ((), (), s32[]{:S(2)}) async-start(), calls=%async_computation.4 | async-start | bytes 4456448 | tf_op jit(solution)/shard_map/all_gather | solution.py:11
  68.8 2.0 copy-start.6
  130.5 7.5 %copy-start.5 = (f32[1,3072,1]{1,2,0:T(1,128)S(1)}, f32[1,3072,1]{1,2,0:T(1,128)}, u32[]{:S(2)}) copy-start(f32[1,3072,1]{1,2,0:T(1,128)} %param.13) | copy-start | bytes 36868
  132.0 30.6 %all-to-all-start = ((bf16[192,16,192]{0,2,1:T(8,128)(2,1)}), bf16[192,16,192]{0,2,1:T(8,128)(2,1)S(1)}, u32[]{:S(2)}, u32[]{:S(2)}) async-start(bf16[192,16,192]{0,2,1:T(8,128)(2,1)} %pad_maximum_fusion), calls=%async_computation | async-start | bytes 3145728 | tf_op jit(solution)/shard_map/all_to_all | solution.py:34
  137.2 206.4 %all-gather.7.cloned.1.call-start = ((), (), s32[]{:S(2)}) async-start(), calls=%async_computation.3 | async-start | bytes 4456448 | tf_op jit(solution)/shard_map/all_gather | solution.py:101
  165.2 18.6 %copy-start.1 = (bf16[3072,1,192]{0,2,1:T(8,128)(2,1)}, bf16[3072,1,192]{0,2,1:T(8,128)(2,1)S(1)}, u32[]{:S(2)}) copy-start(bf16[3072,1,192]{0,2,1:T(8,128)(2,1)S(1)} %all_to_all.27) | copy-start | bytes 3538948
  278.9 14.8 %copy-start.3 = (f32[2048,512]{1,0:T(8,128)S(1)}, f32[2048,512]{1,0:T(8,128)}, u32[]{:S(2)}) copy-start(f32[2048,512]{1,0:T(8,128)} %get-tuple-element.16) | copy-start | bytes 12582916
  281.5 19.6 %slice-start.2 = ((s8[5242880]{0:T(1024)(128)(4,1)}), s8[4194304]{0:T(1024)(128)(4,1)S(1)}, s32[]{:S(2)}) async-start(s8[5242880]{0:T(1024)(128)(4,1)} %bitcast.411), calls=%async_computation.7 | async-start | bytes 8388608
  287.3 6.4 %copy-start = (f32[1,512,16,128]{1,3,2,0:T(8,128)S(1)}, f32[1,512,16,128]{1,3,2,0:T(8,128)}, u32[]{:S(2)}) copy-start(f32[1,512,16,128]{1,3,2,0:T(8,128)} %copy.87) | copy-start | bytes 12582916
  287.3 13.8 %slice-start.3 = ((s8[5242880]{0:T(1024)(128)(4,1)}), s8[1048576]{0:T(1024)(128)(4,1)S(1)}, s32[]{:S(2)}) async-start(s8[5242880]{0:T(1024)(128)(4,1)} %bitcast.411), calls=%async_computation.8 | async-start | bytes 2097152
  293.7 17.3 %slice-start = ((s8[6291456]{0:T(1024)(128)(4,1)}), s8[4194304]{0:T(1024)(128)(4,1)S(1)}, s32[]{:S(2)}) async-start(s8[6291456]{0:T(1024)(128)(4,1)} %bitcast.409), calls=%async_computation.5 | async-start | bytes 8388608
  293.7 17.3 %slice-start.4 = ((s8[6291456]{0:T(1024)(128)(4,1)}), s8[2097152]{0:T(1024)(128)(4,1)S(1)}, s32[]{:S(2)}) async-start(s8[6291456]{0:T(1024)(128)(4,1)} %bitcast.414), calls=%async_computation.9 | async-start | bytes 4194304
  301.1 9.9 %slice-start.1 = ((s8[6291456]{0:T(1024)(128)(4,1)}), s8[2097152]{0:T(1024)(128)(4,1)S(1)}, s32[]{:S(2)}) async-start(s8[6291456]{0:T(1024)(128)(4,1)} %bitcast.409), calls=%async_computation.6 | async-start | bytes 4194304
  301.1 9.9 %slice-start.5 = ((s8[6291456]{0:T(1024)(128)(4,1)}), s8[4194304]{0:T(1024)(128)(4,1)S(1)}, s32[]{:S(2)}) async-start(s8[6291456]{0:T(1024)(128)(4,1)} %bitcast.414), calls=%async_computation.10 | async-start | bytes 8388608
  311.1 10.9 %copy-start.2 = (bf16[3072,1,192]{0,2,1:T(8,128)(2,1)S(1)}, bf16[3072,1,192]{0,2,1:T(8,128)(2,1)}, u32[]{:S(2)}) copy-start(bf16[3072,1,192]{0,2,1:T(8,128)(2,1)} %copy-done.1) | copy-start | bytes 3538948
Sparse Core Ops, SparseCore 0:
  21.9 46.8 all-gather.4
  70.9 50.7 all-gather.8
  140.2 54.9 all-gather.6
